TPU v7x, 1024 devices: a whole 4x8x16 slice. The times are simulated.
1024 devices in a mesh: ep: 32 (over z, core), tp: 32 (over y, x).
Axes of the slice: x: 4, y: 8, z: 16, core: 2. Of those that a mesh axis runs over, the one named last changes fastest.
Arguments:
- tokens: bfloat16 [4096, 4096], P('ep', 'tp'), may hold values from -6 to 6
- routes: int32 [4096, 2], P('ep'), may hold values from 0 to 63, all different within a row; in each aligned block of 128 rows (0 to 127, 128 to 255, ...) at most 5 rows name the same one
- route_weights: float32 [4096, 2], P('ep'), may hold values from 0.2 to 2
- cotangent: bfloat16 [4096, 4096], P('ep', 'tp'), may hold values from -6 to 6
- expert_gate: bfloat16 [64, 4096, 512], P('ep', 'tp'), may hold values from -0.09375 to 0.09375
- expert_up: bfloat16 [64, 4096, 512], P('ep', 'tp'), may hold values from -0.09375 to 0.09375
- expert_down: bfloat16 [64, 512, 4096], P('ep', None, 'tp'), may hold values from -0.25 to 0.25
- shared_gate: bfloat16 [4096, 512], P('tp'), may hold values from -0.09375 to 0.09375
- shared_up: bfloat16 [4096, 512], P('tp'), may hold values from -0.09375 to 0.09375
- shared_down: bfloat16 [512, 4096], P(None, 'tp'), may hold values from -0.25 to 0.25
Outputs:
- grad_tokens: bfloat16 [4096, 4096], P('ep', 'tp')
- grad_weights: float32 [4096, 2], P('ep')
- grad_expert_gate: float32 [64, 4096, 512], P('ep', 'tp')
- grad_expert_up: float32 [64, 4096, 512], P('ep', 'tp')
- grad_expert_down: float32 [64, 512, 4096], P('ep', None, 'tp')
- grad_shared_gate: float32 [4096, 512], P('tp', 'ep')
- grad_shared_up: float32 [4096, 512], P('tp', 'ep')
- grad_shared_down: float32 [512, 4096], P('ep', 'tp')
Inputs may be any that keep to these rules, and one draw needn't show every extreme that they name: `routes`: each row names 2 different experts. In each aligned block of 128 rows (the rows of one index of ep) no expert is named by more than 5 rows, a bound that some block reaches.
All inputs are finite; a program needn't handle non-finite values.
Results may differ from a plain program's by a relative error of at most 0.0054.
Values may be sent and summed in bfloat16 or wider, within the bound.
No kernel may reach another device: no remote copies, remote signals or barrier semaphores. Data moves between devices by JAX's collectives and lax.ppermute only.
A program may use at most 32 MiB of HBM per device.

v0:
```python
import math

import jax
import jax.numpy as jnp
from jax import lax
from jax.sharding import PartitionSpec as P


def sent_together(arrays, axis, dim, along):
    ends, at = ([], 0)
    for a in arrays[:-1]:
        at += a.shape[along]
        ends.append(at)
    both = jnp.concatenate(arrays, axis=along)
    return tuple(
        jnp.split(lax.psum_scatter(both, axis, scatter_dimension=dim, tiled=True), ends, axis=along)
    )


def in_one_piece(arrays, axis, split_dim, concat_dim, along):
    widths = [math.prod(a.shape[along:]) for a in arrays]
    both = jnp.concatenate(
        [a.reshape(*a.shape[:along], w) for a, w in zip(arrays, widths)], axis=along
    )
    result = lax.all_to_all(both, axis, split_axis=split_dim, concat_axis=concat_dim, tiled=True)
    blocks = jnp.split(result, [sum(widths[:k]) for k in range(1, len(widths))], axis=along)
    return tuple(
        (b.reshape(*result.shape[:along], *a.shape[along:]) for a, b in zip(arrays, blocks))
    )


def together(arrays, axis):
    flat, at, done = (jnp.concatenate([a.reshape(-1) for a in arrays]), 0, [])
    running = lax.psum(flat, axis)
    for a in arrays:
        done.append(running[at : at + a.size].reshape(a.shape))
        at += a.size
    return tuple(done)


def cut_along(array, dim, count):
    before, after = (array.shape[:dim], array.shape[dim + 1 :])
    return jnp.moveaxis(array.reshape(*before, count, -1, *after), dim, 0)


def sent_and_summed(array, axis, dim):
    count = lax.axis_size(axis)
    blocks = lax.all_to_all(cut_along(array, dim, count), axis, 0, 0, tiled=True)
    return jnp.sum(blocks, axis=0)


def sent_together_2(arrays, axis, dim, along):
    both = jnp.concatenate(arrays, axis=along)
    result, at, done = (sent_and_summed(both, axis, dim), 0, [])
    for a in arrays:
        done.append(lax.slice_in_dim(result, at, at + a.shape[along], axis=along))
        at += a.shape[along]
    return tuple(done)


def gather_turned(arrays, axis, dims):
    turned = [jnp.moveaxis(a, dim, 0) for a, dim in zip(arrays, dims)]
    both = jnp.concatenate([t.reshape(len(t), -1) for t in turned], axis=1)
    result, at, done = (lax.all_gather(both, axis, axis=0, tiled=True), 0, [])
    for t, dim in zip(turned, dims):
        slab = result[:, at : at + t[0].size].reshape(-1, *t.shape[1:])
        done.append(jnp.moveaxis(slab, 0, dim))
        at += t[0].size
    return tuple(done)


def hidden_terms(gate_pre, up_pre, back_grad, scaling):
    logistic = jax.nn.sigmoid(gate_pre)
    product = gate_pre * logistic * up_pre
    grad_act = scaling * back_grad
    gate_grad = (grad_act * up_pre * logistic * (1.0 + gate_pre * (1.0 - logistic))).astype(
        jnp.bfloat16
    )
    up_grad = (grad_act * gate_pre * logistic).astype(jnp.bfloat16)
    hidden = (scaling * product).astype(jnp.bfloat16)
    return (gate_grad, up_grad, hidden, jnp.sum(back_grad * product, axis=-1))


def shared_weight_sums(tokens, cotangent, shared_gate_grad, shared_up_grad, shared_hidden):
    local_gate = jnp.einsum(
        "td,tf->df", tokens, shared_gate_grad, preferred_element_type=jnp.float32
    )
    local_up = jnp.einsum("td,tf->df", tokens, shared_up_grad, preferred_element_type=jnp.float32)
    local_down = jnp.einsum(
        "tf,td->fd", shared_hidden, cotangent, preferred_element_type=jnp.float32
    )
    return (
        *sent_together((local_gate, local_up), "ep", 1, 0),
        lax.psum_scatter(local_down, "ep", scatter_dimension=0, tiled=True),
    )


def body(
    tokens,
    routes,
    route_weights,
    cotangent,
    expert_gate,
    expert_up,
    expert_down,
    shared_gate,
    shared_up,
    shared_down,
):
    tok_rows, top_count = routes.shape
    feat_cols = tokens.shape[1]
    local_experts = expert_gate.shape[0]
    group_size = lax.axis_size("ep")
    capacity = max(2, 5 * tok_rows * top_count // (4 * group_size * local_experts))
    all_experts = group_size * local_experts
    picked = routes.reshape(-1)
    onehot = (picked[:, None] == jnp.arange(all_experts, dtype=jnp.int32)[None, :]).astype(
        jnp.int32
    )
    ranked = jnp.sum(jnp.cumsum(onehot, axis=0) * onehot, axis=1) - 1
    slot_ids = picked * capacity + ranked
    places = (
        jnp.arange(all_experts * capacity, dtype=jnp.int32)[:, None] == slot_ids[None, :]
    ).astype(jnp.bfloat16)
    repeat_tokens = jnp.repeat(tokens, top_count, axis=0)
    repeat_cotan = jnp.repeat(cotangent, top_count, axis=0)
    gate_bf = route_weights.reshape(-1).astype(jnp.bfloat16)
    send_tokens = jnp.dot(places, repeat_tokens, preferred_element_type=jnp.float32).astype(
        jnp.bfloat16
    )
    send_cotan = jnp.dot(places, repeat_cotan, preferred_element_type=jnp.float32).astype(
        jnp.bfloat16
    )
    send_gates = jnp.dot(places, gate_bf, preferred_element_type=jnp.float32).astype(jnp.bfloat16)
    send_tokens = send_tokens.reshape(group_size, local_experts, capacity, feat_cols)
    send_cotan = send_cotan.reshape(group_size, local_experts, capacity, feat_cols)
    send_gates = send_gates.reshape(group_size, local_experts, capacity)
    got_tokens, got_cotan, got_gates = in_one_piece(
        (send_tokens, send_cotan, send_gates), "ep", 0, 2, 3
    )
    slot_tokens = got_tokens[0]
    slot_cotan = got_cotan[0]
    slot_gates = got_gates[0].astype(jnp.float32)
    part_gate = jnp.einsum(
        "esd,edf->esf", slot_tokens, expert_gate, preferred_element_type=jnp.float32
    )
    part_up = jnp.einsum("esd,edf->esf", slot_tokens, expert_up, preferred_element_type=jnp.float32)
    part_down = jnp.einsum(
        "esd,efd->esf", slot_cotan, expert_down, preferred_element_type=jnp.float32
    )
    gate_pre, up_pre, back_grad = together((part_gate, part_up, part_down), "tp")
    gate_grad, up_grad, hidden, slot_dg = hidden_terms(
        gate_pre, up_pre, back_grad, slot_gates[:, :, None]
    )
    shared_part_gate = jnp.dot(tokens, shared_gate, preferred_element_type=jnp.float32)
    shared_part_up = jnp.dot(tokens, shared_up, preferred_element_type=jnp.float32)
    shared_part_down = jnp.einsum(
        "td,fd->tf", cotangent, shared_down, preferred_element_type=jnp.float32
    )
    share_gate_pre, share_up_pre, share_back = sent_together_2(
        (shared_part_gate, shared_part_up, shared_part_down), "tp", 1, 0
    )
    share_gate_grad, share_up_grad, share_hidden, unused_sum = hidden_terms(
        share_gate_pre, share_up_pre, share_back, 1.0
    )
    shared_gate_grad, shared_up_grad, shared_hidden = gather_turned(
        (share_gate_grad, share_up_grad, share_hidden), "tp", (1, 1, 1)
    )
    slot_grad = jnp.einsum(
        "esf,edf->esd", gate_grad, expert_gate, preferred_element_type=jnp.float32
    ) + jnp.einsum("esf,edf->esd", up_grad, expert_up, preferred_element_type=jnp.float32)
    grad_expert_gate = jnp.einsum(
        "esd,esf->edf", slot_tokens, gate_grad, preferred_element_type=jnp.float32
    )
    grad_expert_up = jnp.einsum(
        "esd,esf->edf", slot_tokens, up_grad, preferred_element_type=jnp.float32
    )
    grad_expert_down = jnp.einsum(
        "esf,esd->efd", hidden, slot_cotan, preferred_element_type=jnp.float32
    )
    back_rows, back_dg = in_one_piece((slot_grad, slot_dg), "ep", 1, 0, 2)
    back_rows = back_rows.reshape(all_experts * capacity, feat_cols)
    back_dg = back_dg.reshape(all_experts * capacity)
    routed_grad = jnp.sum(
        jnp.take(back_rows, slot_ids, axis=0).reshape(tok_rows, top_count, feat_cols), axis=1
    )
    grad_weights = jnp.take(back_dg, slot_ids).reshape(tok_rows, top_count)
    shared_grad = jnp.einsum(
        "tf,df->td", shared_gate_grad, shared_gate, preferred_element_type=jnp.float32
    ) + jnp.einsum("tf,df->td", shared_up_grad, shared_up, preferred_element_type=jnp.float32)
    grad_shared_gate, grad_shared_up, grad_shared_down = shared_weight_sums(
        tokens, cotangent, shared_gate_grad, shared_up_grad, shared_hidden
    )
    grad_tokens = (routed_grad + shared_grad).astype(jnp.bfloat16)
    return (
        grad_tokens,
        grad_weights,
        grad_expert_gate,
        grad_expert_up,
        grad_expert_down,
        grad_shared_gate,
        grad_shared_up,
        grad_shared_down,
    )


def solution(mesh):
    return jax.shard_map(
        body,
        mesh=mesh,
        in_specs=(
            P("ep", "tp"),
            P("ep", None),
            P("ep", None),
            P("ep", "tp"),
            P("ep", "tp", None),
            P("ep", "tp", None),
            P("ep", None, "tp"),
            P("tp", None),
            P("tp", None),
            P(None, "tp"),
        ),
        out_specs=(
            P("ep", "tp"),
            P("ep", None),
            P("ep", "tp", None),
            P("ep", "tp", None),
            P("ep", None, "tp"),
            P("tp", "ep"),
            P("tp", "ep"),
            P("ep", "tp"),
        ),
        check_vma=False,
    )
```

profile of v0, /device:TPU:1, one launch (start us, length us, event | category | flops | bytes accessed | tf_op | source)
XLA Modules:
  0.0 377.2 jit_solution(10246408110979146032)
XLA Ops:
  15.3 20.4 %all-to-all-start = ((bf16[32,2,5,257]{3,1,2,0:T(2,128)(2,1)}), bf16[32,2,5,257]{3,1,2,0:T(2,128)(2,1)S(1)}, u32[]{:S(2)}, u32[]{:S(2)}) async-start(bf16[32,2,5,257]{3,1,2,0:T(2,128)(2,1)} %copy.66), calls=%async_computation | async-start | bytes 491520 | tf_op jit(solution)/shard_map/all_to_all | solution.py:25
  36.3 1.2 copy.74
  37.5 19.2 %all-to-all-done = bf16[32,2,5,257]{3,1,2,0:T(2,128)(2,1)S(1)} async-done(((bf16[32,2,5,257]{3,1,2,0:T(2,128)(2,1)}), bf16[32,2,5,257]{3,1,2,0:T(2,128)(2,1)S(1)}, u32[]{:S(2)}, u32[]{:S(2)}) %all-to-all-start) | async-done | bytes 164512 | tf_op jit(solution)/shard_map/all_to_all | solution.py:25
  56.7 9.8 %all-to-all-start.2 = ((f32[32,384,16]{1,2,0:T(8,128)}), f32[32,384,16]{1,2,0:T(8,128)S(1)}, u32[]{:S(2)}, u32[]{:S(2)}) async-start(f32[32,384,16]{1,2,0:T(8,128)} %bitcast.18), calls=%async_computation.2 | async-start | bytes 1572864 | tf_op jit(solution)/shard_map/all_to_all | solution.py:48
  68.3 18.9 %all-to-all-done.2 = f32[32,384,16]{1,2,0:T(8,128)S(1)} async-done(((f32[32,384,16]{1,2,0:T(8,128)}), f32[32,384,16]{1,2,0:T(8,128)S(1)}, u32[]{:S(2)}, u32[]{:S(2)}) %all-to-all-start.2) | async-done | bytes 786464 | tf_op jit(solution)/shard_map/all_to_all | solution.py:48
  87.3 37.0 %all_gather.3 = bf16[512,384]{1,0:T(8,128)(2,1)S(1)} all-gather(bf16[16,384]{1,0:T(8,128)(2,1)S(1)} %pad_maximum_fusion.5), channel_id=1, replica_groups=mesh['ep'=32,'tp'=32] {'tp'}, dimensions={0}, use_global_device_ids=true | all-gather | bytes 405504 | tf_op jit(solution)/shard_map/all_gather | solution.py:64
  124.3 1.0 convolution_bitcast_fusion
  125.3 1.0 convolution_bitcast_fusion.1
  126.3 1.0 copy.79
  127.4 1.4 pad_maximum_fusion
  130.2 0.9 split.28
  133.0 108.2 %reduce-scatter.7.cloned.1.call-done = f32[16,256]{1,0:T(8,128)} async-done(((f32[512,256]{1,0:T(8,128)}), f32[16,256]{1,0:T(8,128)}) %reduce-scatter.7.cloned.1.call-update) | async-done | bytes 16400
  241.2 1.3 fusion.27
  242.5 71.8 %all-reduce.2.cloned.1.call-done = f32[491520]{0:T(1024)} async-done(((f32[491520]{0:T(1024)}), f32[491520]{0:T(1024)}) %all-reduce.2.cloned.1.call-update) | async-done | bytes 1966096 | tf_op jit(solution)/shard_map/psum | solution.py:34
  314.3 1.6 fusion.25
  316.2 1.8 multiply_convert_fusion.2
  319.1 1.2 convolution_add_fusion
  320.3 1.0 copy.71
  321.3 17.4 %all-to-all-start.1 = ((f32[2,160,129]{2,0,1:T(2,128)}), f32[2,160,129]{2,0,1:T(2,128)S(1)}, u32[]{:S(2)}, u32[]{:S(2)}) async-start(f32[2,160,129]{2,0,1:T(2,128)} %copy.71), calls=%async_computation.1 | async-start | bytes 655360 | tf_op jit(solution)/shard_map/all_to_all | solution.py:25
  338.8 1.1 fusion.18
  339.8 1.1 fusion.19
  340.9 1.3 fusion.2
  342.2 21.8 %all-to-all-done.1 = f32[2,160,129]{2,0,1:T(2,128)S(1)} async-done(((f32[2,160,129]{2,0,1:T(2,128)}), f32[2,160,129]{2,0,1:T(2,128)S(1)}, u32[]{:S(2)}, u32[]{:S(2)}) %all-to-all-start.1) | async-done | bytes 165152 | tf_op jit(solution)/shard_map/all_to_all | solution.py:25
  365.0 1.9 gather_fusion.1
  (108 shorter events, 18.0 us)
Async XLA Ops:
  8.0 58.7 %copy-start = (bf16[2,128,512]{2,1,0:T(8,128)(2,1)S(1)}, bf16[2,128,512]{2,1,0:T(8,128)(2,1)}, u32[]{:S(2)}) copy-start(bf16[2,128,512]{2,1,0:T(8,128)(2,1)} %param.14) | copy-start | bytes 786436
  8.0 27.7 %copy-start.3 = (bf16[128,128]{1,0:T(8,128)(2,1)S(1)}, bf16[128,128]{1,0:T(8,128)(2,1)}, u32[]{:S(2)}) copy-start(bf16[128,128]{1,0:T(8,128)(2,1)} %param.10) | copy-start | bytes 98308
  8.0 27.7 %copy-start.4 = (bf16[128,512]{1,0:T(8,128)(2,1)S(1)}, bf16[128,512]{1,0:T(8,128)(2,1)}, u32[]{:S(2)}) copy-start(bf16[128,512]{1,0:T(8,128)(2,1)} %param.17) | copy-start | bytes 393220
  9.2 26.7 %copy-start.6 = (bf16[128,512]{1,0:T(8,128)(2,1)S(1)}, bf16[128,512]{1,0:T(8,128)(2,1)}, u32[]{:S(2)}) copy-start(bf16[128,512]{1,0:T(8,128)(2,1)} %param.18) | copy-start | bytes 393220
  11.5 24.6 %copy-start.10 = (bf16[128,128]{1,0:T(8,128)(2,1)S(1)}, bf16[128,128]{1,0:T(8,128)(2,1)}, u32[]{:S(2)}) copy-start(bf16[128,128]{1,0:T(8,128)(2,1)} %param.13) | copy-start | bytes 98308
  11.5 24.6 %copy-start.13 = (bf16[512,128]{1,0:T(8,128)(2,1)S(1)}, bf16[512,128]{1,0:T(8,128)(2,1)}, u32[]{:S(2)}) copy-start(bf16[512,128]{1,0:T(8,128)(2,1)} %param.19) | copy-start | bytes 393220
  15.3 41.4 %all-to-all-start = ((bf16[32,2,5,257]{3,1,2,0:T(2,128)(2,1)}), bf16[32,2,5,257]{3,1,2,0:T(2,128)(2,1)S(1)}, u32[]{:S(2)}, u32[]{:S(2)}) async-start(bf16[32,2,5,257]{3,1,2,0:T(2,128)(2,1)} %copy.66), calls=%async_computation | async-start | bytes 491520 | tf_op jit(solution)/shard_map/all_to_all | solution.py:25
  56.7 10.0 %copy-start.2 = (bf16[32,2,5,257]{3,1,2,0:T(2,128)(2,1)}, bf16[32,2,5,257]{3,1,2,0:T(2,128)(2,1)S(1)}, u32[]{:S(2)}) copy-start(bf16[32,2,5,257]{3,1,2,0:T(2,128)(2,1)S(1)} %all-to-all-done) | copy-start | bytes 493444
  56.7 10.4 %copy-start.1 = (bf16[2,128,512]{2,1,0:T(8,128)(2,1)S(1)}, bf16[2,128,512]{2,1,0:T(8,128)(2,1)}, u32[]{:S(2)}) copy-start(bf16[2,128,512]{2,1,0:T(8,128)(2,1)} %param.15) | copy-start | bytes 786436
  56.7 30.5 %all-to-all-start.2 = ((f32[32,384,16]{1,2,0:T(8,128)}), f32[32,384,16]{1,2,0:T(8,128)S(1)}, u32[]{:S(2)}, u32[]{:S(2)}) async-start(f32[32,384,16]{1,2,0:T(8,128)} %bitcast.18), calls=%async_computation.2 | async-start | bytes 1572864 | tf_op jit(solution)/shard_map/all_to_all | solution.py:48
  66.5 174.7 %reduce-scatter.7.cloned.1.call-start = ((), (), s32[]{:S(2)}) async-start(), calls=%async_computation.7 | async-start | bytes 540672
  66.7 0.9 copy-start.8
  66.9 1.0 copy-start.12
  127.4 186.9 %all-reduce.2.cloned.1.call-start = ((), (), s32[]{:S(2)}) async-start(), calls=%async_computation.5 | async-start | bytes 3932160 | tf_op jit(solution)/shard_map/psum | solution.py:34
  128.8 0.7 copy-start.14
  128.8 3.1 copy-start.5
  128.8 3.3 copy-start.11
  128.8 240.9 %reduce-scatter.5.cloned.1.call-start = ((), (), s32[]{:S(2)}) async-start(), calls=%async_computation.6 | async-start | bytes 270336 | tf_op jit(solution)/shard_map/reduce_scatter | solution.py:94
  320.3 20.6 %copy-start.9 = (bf16[1,2,160,128]{3,1,2,0:T(2,128)(2,1)S(1)}, bf16[1,2,160,128]{3,1,2,0:T(2,128)(2,1)}, u32[]{:S(2)}) copy-start(bf16[1,2,160,128]{3,1,2,0:T(2,128)(2,1)} %copy-done.8) | copy-start | bytes 245764
  320.3 20.6 %copy-start.16 = (f32[2,160]{1,0:T(2,128)S(1)}, f32[2,160]{1,0:T(2,128)}, u32[]{:S(2)}) copy-start(f32[2,160]{1,0:T(2,128)} %bitcast_convert_fusion) | copy-start | bytes 3844
  321.3 42.6 %all-to-all-start.1 = ((f32[2,160,129]{2,0,1:T(2,128)}), f32[2,160,129]{2,0,1:T(2,128)S(1)}, u32[]{:S(2)}, u32[]{:S(2)}) async-start(f32[2,160,129]{2,0,1:T(2,128)} %copy.71), calls=%async_computation.1 | async-start | bytes 655360 | tf_op jit(solution)/shard_map/all_to_all | solution.py:25
  340.9 24.1 %copy-start.15 = (s32[1024]{0:T(1024)S(1)}, s32[1024]{0:T(1024)}, u32[]{:S(2)}) copy-start(s32[1024]{0:T(1024)} %pad_clamp_fusion) | copy-start | bytes 12292
  364.3 4.5 %copy-start.7 = (bf16[128,512]{1,0:T(8,128)(2,1)S(1)}, bf16[128,512]{1,0:T(8,128)(2,1)}, u32[]{:S(2)}) copy-start(bf16[128,512]{1,0:T(8,128)(2,1)} %param.18) | copy-start | bytes 393220
Sparse Core Ops, SparseCore 0:
  127.5 113.6 reduce-scatter.6
  245.2 112.3 reduce-scatter.4
Sparse Core Ops, SparseCore 1:
  131.3 182.9 all-reduce.1
where the time goes:
time: 378 us; the launch traced here: 377 us
  waiting for transfers between devices  240 us (63%)
  starting transfers between devices  47.8 us (13%)
  blocking collectives  37 us (10%)
  local copies, waits for them, and re-layouts  19 us (5%)
  between operations  16 us (4%)
  matrix products  10.5 us (3%)
  other arithmetic  6.98 us (2%)
    unnamed x4, waiting for transfers between devices  108 us
    psum x1, waiting for transfers between devices, together(): running = lax.psum(flat, axis)  71.8 us
    all_to_all x2, waiting for transfers between devices, in_one_piece(): lax.all_to_all(both, axis, split_axis=split_dim, concat_axis=concat_dim,...  40.9 us
    all_to_all x2, starting transfers between devices, in_one_piece(): lax.all_to_all(both, axis, split_axis=split_dim, concat_axis=concat_dim,...  37.8 us
    all_gather x1, blocking collectives, gather_turned(): result, at, done = (lax.all_gather(both, axis, axis=0, tiled=True), 0, [])  37 us
    all_to_all x1, waiting for transfers between devices, sent_and_summed(): lax.all_to_all(cut_along(array, dim, count), axis, 0, 0, tiled=True)  18.9 us
    all_to_all x1, starting transfers between devices, sent_and_summed(): lax.all_to_all(cut_along(array, dim, count), axis, 0, 0, tiled=True)  9.8 us
  transfers between devices with their start and end apart: 6, of which 5 were waited for; matrix products, arithmetic and copies ran while one was open for 7% of the time, Pallas kernels for 0%

commit v1 on v0

v1 whole, which is shorter than its diff:
```python
import jax
import jax.numpy as jnp
from jax import lax
from jax.experimental import pallas as pl
from jax.experimental.pallas import tpu as pltpu
from jax.sharding import Mesh
from jax.sharding import PartitionSpec as P

BF, F32, I32 = jnp.bfloat16, jnp.float32, jnp.int32
NZ, NC, NY, NX = 16, 2, 8, 4
NEP, NTP = NZ * NC, NY * NX
CAP, BLK = 5, 16
SLOTS = 2 * CAP
SHR = 4
USED = SLOTS + SHR
XROWS = NY * USED
HID = 512


def iota(shape, dim):
    return lax.broadcasted_iota(I32, shape, dim)


def nn(a, b):
    return jnp.dot(a, b, preferred_element_type=F32)


def nt(a, b):
    return lax.dot_general(a, b, (((1,), (1,)), ((), ())), preferred_element_type=F32)


def tn(a, b):
    return lax.dot_general(a, b, (((0,), (0,)), ((), ())), preferred_element_type=F32)


def onehot(cond):
    return jnp.where(cond, 1.0, 0.0).astype(BF)


def call(kernel, outs):
    def run(*args):
        return pl.pallas_call(
            kernel,
            out_shape=outs,
            in_specs=[pl.BlockSpec(memory_space=pltpu.VMEM)] * len(args),
            out_specs=jax.tree.map(lambda _: pl.BlockSpec(memory_space=pltpu.VMEM), outs),
        )(*args)

    return run


def struct(shape, dtype):
    return jax.ShapeDtypeStruct(shape, dtype)


def route_kernel(routes, weights, tok, cot, send, ids):
    n = tok.shape[0]
    r0, r1 = routes[:, 0:1], routes[:, 1:2]
    lane = iota((n, 128), 1)
    oh0, oh1 = r0 == lane, r1 == lane
    earlier = onehot(iota((n, n), 0) > iota((n, n), 1))
    f0, f1 = jnp.where(oh0, 1.0, 0.0), jnp.where(oh1, 1.0, 0.0)
    c0 = nn(earlier, f0.astype(BF))
    c1 = nn(earlier, f1.astype(BF)) + jnp.sum(f0, axis=0, keepdims=True)
    rank0 = jnp.sum(c0 * f0, axis=1, keepdims=True).astype(I32)
    rank1 = jnp.sum(c1 * f1, axis=1, keepdims=True).astype(I32)
    row0 = (r0 >> 1) * BLK + (r0 & 1) * CAP + rank0
    row1 = (r1 >> 1) * BLK + (r1 & 1) * CAP + rank1
    ids[...] = jnp.where(iota((n, 2), 1) == 0, row0, row1)
    wide = iota((n, NEP * BLK), 1)
    places = onehot((row0 == wide) | (row1 == wide))
    at0 = onehot((row0 >> 4) * BLK + SLOTS == wide)
    at1 = onehot((row1 >> 4) * BLK + SLOTS == wide)
    gates = weights[...].astype(BF).astype(F32)
    lane2 = iota((n, 256), 1)
    g0 = jnp.where(lane2 == (row0 & 15), gates[:, 0:1], 0.0).astype(BF)
    g1 = jnp.where(lane2 == (row1 & 15), gates[:, 1:2], 0.0).astype(BF)
    feats = jnp.concatenate([tok[...], cot[...]], axis=1)
    left = jnp.concatenate([places, at0, at1], axis=0)
    right = jnp.concatenate([feats, g0, g1], axis=0)
    send[...] = tn(left, right).astype(BF)


def partial_kernel(recv, tok, cot, wg, wu, wd, sg, su, sd, out):
    rows = NX * XROWS
    r = iota((rows, 1), 0)
    x = (r * 293) >> 15
    rest = r - x * XROWS
    y = (rest * 293) >> 12
    q = rest - y * USED
    s = y * NX + x
    src = jnp.where(q < SLOTS, s * BLK + q, NEP * BLK + s * SHR + q - SLOTS)
    pick = onehot(src == iota((rows, NEP * BLK + 128), 1))
    feats = jnp.concatenate([tok[...], cot[...]], axis=1)
    data = nn(pick, jnp.concatenate([recv[...], feats], axis=0))
    kinds = (q < CAP, (q >= CAP) & (q < SLOTS), q >= SLOTS)
    t, c = data[:, :128], data[:, 128:]
    tcat = jnp.concatenate([jnp.where(k, t, 0.0).astype(BF) for k in kinds], axis=1)
    ccat = jnp.concatenate([jnp.where(k, c, 0.0).astype(BF) for k in kinds], axis=1)
    wgc = jnp.concatenate([wg[0], wg[1], sg[...]], axis=0)
    out[:, :HID] = nn(tcat, wgc).astype(BF)
    wuc = jnp.concatenate([wu[0], wu[1], su[...]], axis=0)
    out[:, HID : 2 * HID] = nn(tcat, wuc).astype(BF)
    wdc = jnp.concatenate([wd[0], wd[1], sd[...]], axis=1)
    out[:, 2 * HID :] = nt(ccat, wdc).astype(BF)


def middle_kernel(got, out):
    o = iota((NY * BLK, 1), 0)
    q = o & 15
    want = jnp.where(q < USED, (o >> 4) * USED + q, -1)
    r = iota((NY * BLK, XROWS), 1)
    pick = onehot(want == r)
    total = nn(pick, got[0])
    for k in range(1, NX):
        total = total + nn(pick, got[k])
    out[...] = total.astype(BF)


def hidden_kernel(got, recv, out):
    t = lax.axis_index("y") * NX + lax.axis_index("x")
    pre = got[0].astype(F32)
    for k in range(1, NY):
        pre = pre + got[k].astype(F32)
    gate, up, back = pre[:, :HID], pre[:, HID : 2 * HID], pre[:, 2 * HID :]
    q = iota((BLK, 1), 0)
    lane = iota((BLK, 128), 1)
    block = recv[t, :, :128].astype(F32)
    grow = jnp.sum(jnp.where(iota((BLK, 128), 0) == SLOTS, block, 0.0), axis=0, keepdims=True)
    gcol = jnp.sum(jnp.where(lane == iota((BLK, 128), 0), grow, 0.0), axis=1, keepdims=True)
    scale = jnp.where(q < SLOTS, gcol, 1.0)
    logistic = jax.nn.sigmoid(gate)
    product = gate * logistic * up
    grad_act = scale * back
    gate_grad = (grad_act * up * logistic * (1.0 + gate * (1.0 - logistic))).astype(BF)
    up_grad = (grad_act * gate * logistic).astype(BF)
    hidden = (scale * product).astype(BF)
    dg = jnp.sum(back * product, axis=1, keepdims=True)
    lane_h = iota((BLK, HID), 1)
    row_h = iota((BLK, HID), 0)
    line = jnp.sum(jnp.where(lane_h == row_h, dg, 0.0), axis=0, keepdims=True)
    high = line.astype(BF).astype(F32)
    extra = jnp.where(row_h == USED, high, line - high)
    gate_grad = jnp.where(row_h >= USED, extra, gate_grad.astype(F32)).astype(BF)
    for k in range(NY):
        out[k, :, :HID] = gate_grad
        out[k, :, HID : 2 * HID] = up_grad
        out[k, :, 2 * HID :] = hidden


def back_kernel(grads, tok, cot, wg, wu, sg, su, shared_grad, send):
    n = tok.shape[0]
    token = iota((n, 1), 0)
    s = token >> 2
    want = (s & 3) * (NY * BLK) + (s >> 2) * BLK + SLOTS + (token & 3)
    pick = onehot(want == iota((n, NTP * BLK), 1))
    shared = nn(pick, grads[...]).astype(BF)
    shared_grad[...] = nt(shared[:, :HID], sg[...]) + nt(shared[:, HID : 2 * HID], su[...])
    wt = tn(shared[:, : 2 * HID], tok[...]).astype(BF)
    wdn = tn(shared[:, 2 * HID :], cot[...]).astype(BF)
    gg, gu = grads[:, :HID], grads[:, HID : 2 * HID]
    d0 = nt(gg, wg[0]) + nt(gu, wu[0])
    d1 = nt(gg, wg[1]) + nt(gu, wu[1])
    q = iota((NTP * BLK, 1), 0) & 15
    rows = jnp.where(q < CAP, d0, jnp.where(q < SLOTS, d1, gg[:, :128].astype(F32))).astype(BF)
    for y in range(NY):
        for x in range(NX):
            d = y * NX + x
            z, c = d // NC, d % NC
            at = (x * NY + y) * BLK
            send[c, z, 0:BLK] = rows[at : at + BLK]
            send[c, z, BLK : 2 * BLK] = wt[d * BLK : d * BLK + BLK]
            send[c, z, 2 * BLK : 3 * BLK] = wt[HID + d * BLK : HID + d * BLK + BLK]
            send[c, z, 3 * BLK :] = wdn[d * BLK : d * BLK + BLK]


def weights_kernel(grads, recv, og, ou, od):
    blocks = [recv[y * NX + x] for x in range(NX) for y in range(NY)]
    data = jnp.concatenate(blocks, axis=0)
    q = iota((NTP * BLK, 1), 0) & 15
    first = onehot(q < CAP)
    second = onehot((q >= CAP) & (q < SLOTS))
    t, c = data[:, :128], data[:, 128:]
    tcat = jnp.concatenate([t * first, t * second], axis=1)
    ccat = jnp.concatenate([c * first, c * second], axis=1)
    g = tn(tcat, grads[:, :HID])
    og[0], og[1] = g[:128], g[128:]
    u = tn(tcat, grads[:, HID : 2 * HID])
    ou[0], ou[1] = u[:128], u[128:]
    d = tn(grads[:, 2 * HID :], ccat)
    od[0], od[1] = d[:, :128], d[:, 128:]


def core_kernel(got, out):
    for z in range(NZ):
        out[z, :BLK] = got[0, z, :BLK]
        out[z, BLK : 2 * BLK] = got[1, z, :BLK]
        both = got[0, z, BLK:].astype(F32) + got[1, z, BLK:].astype(F32)
        out[z, 2 * BLK :] = both.astype(BF)


def final_kernel(got, ids, shared_grad, grad_tokens, grad_weights, og, ou, od):
    n = ids.shape[0]
    row0, row1 = ids[:, 0:1], ids[:, 1:2]
    back = jnp.concatenate([got[z, : 2 * BLK] for z in range(NZ)], axis=0)
    wide = iota((n, NEP * BLK), 1)
    places = onehot((row0 == wide) | (row1 == wide))
    grad_tokens[...] = (nn(places, back) + shared_grad[...]).astype(BF)
    lane = iota((n, 128), 1)
    sums = []
    for row in (row0, row1):
        base = (row >> 4) * BLK + USED
        line = nn(onehot((wide == base) | (wide == base + 1)), back)
        sums.append(jnp.sum(jnp.where(lane == (row & 15), line, 0.0), axis=1, keepdims=True))
    grad_weights[...] = jnp.where(iota((n, 2), 1) == 0, sums[0], sums[1])
    total = got[0, 2 * BLK :].astype(F32)
    for z in range(1, NZ):
        total = total + got[z, 2 * BLK :].astype(F32)
    od[...] = total[2 * BLK :]
    pad = jnp.zeros((128 - 2 * BLK, 128), F32)
    turned = jnp.concatenate([total[: 2 * BLK], pad], axis=0).T
    og[...] = turned[:, :BLK]
    ou[...] = turned[:, BLK : 2 * BLK]


def swap(array, axis):
    return lax.all_to_all(array, axis, 0, 0, tiled=True)


def body(tok, routes, weights, cot, wg, wu, wd, sg, su, sd):
    n, feats = tok.shape
    send, ids = call(
        route_kernel, (struct((NEP * BLK, 2 * feats), BF), struct((n, 2), I32))
    )(routes, weights, tok, cot)
    recv = swap(send.reshape(NEP, BLK, 2 * feats), ("z", "core"))
    part = call(partial_kernel, struct((NX * XROWS, 3 * HID), BF))(
        recv.reshape(NEP * BLK, 2 * feats), tok, cot, wg, wu, wd, sg, su, sd
    )
    got = swap(part.reshape(NX, XROWS, 3 * HID), "x")
    mid = call(middle_kernel, struct((NY * BLK, 3 * HID), BF))(got)
    got = swap(mid.reshape(NY, BLK, 3 * HID), "y")
    grads = call(hidden_kernel, struct((NY, BLK, 3 * HID), BF))(got, recv)
    grads = swap(grads, "y").reshape(1, NY * BLK, 3 * HID)
    grads = swap(jnp.broadcast_to(grads, (NX, NY * BLK, 3 * HID)), "x")
    grads = grads.reshape(NTP * BLK, 3 * HID)
    shared_grad, back = call(
        back_kernel, (struct((n, feats), F32), struct((NC, NZ, 4 * BLK, feats), BF))
    )(grads, tok, cot, wg, wu, sg, su)
    back = swap(back, "core")
    back = call(core_kernel, struct((NZ, 5 * BLK, feats), BF))(back)
    back = swap(back, "z")
    grad_g, grad_u, grad_d = call(
        weights_kernel,
        (struct((2, feats, HID), F32), struct((2, feats, HID), F32), struct((2, HID, feats), F32)),
    )(grads, recv)
    grad_tokens, grad_weights, shared_g, shared_u, shared_d = call(
        final_kernel,
        (
            struct((n, feats), BF),
            struct((n, 2), F32),
            struct((feats, BLK), F32),
            struct((feats, BLK), F32),
            struct((BLK, feats), F32),
        ),
    )(back, ids, shared_grad)
    return grad_tokens, grad_weights, grad_g, grad_u, grad_d, shared_g, shared_u, shared_d


def solution(mesh):
    ep, tp = ("z", "core"), ("y", "x")
    fine = Mesh(mesh.devices.reshape(NZ, NC, NY, NX), ("z", "core", "y", "x"))
    return jax.shard_map(
        body,
        mesh=fine,
        in_specs=(
            P(ep, tp),
            P(ep, None),
            P(ep, None),
            P(ep, tp),
            P(ep, tp, None),
            P(ep, tp, None),
            P(ep, None, tp),
            P(tp, None),
            P(tp, None),
            P(None, tp),
        ),
        out_specs=(
            P(ep, tp),
            P(ep, None),
            P(ep, tp, None),
            P(ep, tp, None),
            P(ep, None, tp),
            P(tp, ep),
            P(tp, ep),
            P(ep, tp),
        ),
        check_vma=False,
    )
```

time: 378 us -> 184 us (0.49)
  the two profiles are of different devices: /device:TPU:1 before, /device:TPU:2 now
where the time goes in v1:
time: 184 us; the launch traced here: 183 us
  blocking collectives  128 us (70%)
  Pallas kernels  21.4 us (12%)
  waiting for transfers between devices  18.5 us (10%)
  local copies, waits for them, and re-layouts  8.17 us (4%)
  starting transfers between devices  6.04 us (3%)
    all_to_all x6, blocking collectives, swap(): return lax.all_to_all(array, axis, 0, 0, tiled=True)  128 us
    pallas_call x8, Pallas kernels, run(): pl.pallas_call(kernel, out_shape=outs, in_specs=[pl.BlockSpec(memory_spac...  21.4 us
    all_to_all x1, waiting for transfers between devices, swap(): return lax.all_to_all(array, axis, 0, 0, tiled=True)  18.5 us
    unnamed x7, local copies, waits for them, and re-layouts  8.05 us
    all_to_all x1, starting transfers between devices, swap(): return lax.all_to_all(array, axis, 0, 0, tiled=True)  6.04 us
  transfers between devices with their start and end apart: 1, of which 1 were waited for; matrix products, arithmetic and copies ran while one was open for 0% of the time, Pallas kernels for 2%

profile of v1, /device:TPU:2, one launch (start us, length us, event | category | flops | bytes accessed | tf_op | source)
XLA Modules:
  0.0 182.7 jit_solution(1282407492509131192)
XLA Ops:
  0.6 1.4 copy.18.routes
  2.0 1.4 copy.19.weights
  3.5 2.4 %shard_map.161 = (bf16[512,256]{1,0:T(8,128)(2,1)}, s32[128,2]{1,0:T(8,128)}) custom-call(s32[128,2]{1,0:T(8,128)} %copy.18.routes, f32[128,2]{1,0:T(8,128)} %copy.19.weights, bf16[128,128]{1,0:T(8,128)(2,1)} %tok.5, bf16[128,128]{1,0:T(8,128)(2,1)} %cot.5), custom_call_target="tpu_custom_call" | custom-call | tf_op jit(solution)/shard_map/pallas_call | solution.py:42
  5.9 41.9 %all_to_all.35.recv = bf16[32,16,256]{2,1,0:T(8,128)(2,1)} all-to-all(bf16[32,16,256]{2,1,0:T(8,128)(2,1)} %bitcast.12), channel_id=1, replica_groups=mesh['z'=16,'core'=2,'y'=8,'x'=4] {'z','core'}, dimensions={0} | all-to-all | bytes 524288 | tf_op jit(solution)/shard_map/all_to_all | solution.py:227
  47.8 3.9 %shard_map.162 = bf16[448,1536]{1,0:T(8,128)(2,1)} custom-call(bf16[512,256]{1,0:T(8,128)(2,1)} %bitcast.9, bf16[128,128]{1,0:T(8,128)(2,1)} %tok.5, bf16[128,128]{1,0:T(8,128)(2,1)} %cot.5, bf16[2,128,512]{2,1,0:T(8,128)(2,1)} %wg.3, bf16[2,128,512]{2,1,0:T(8,128)(2,1)} %wu.3, bf16[2,512,128]{2,1,0:T(8,128)(2,1)} %wd.1, bf16[128,512]{1,0:T(8,128)(2,1)} %sg.3, ...), custom_call_target="tpu_custom_call" | custom-call | tf_op jit(solution)/shard_map/pallas_call | solution.py:42
  51.7 22.4 %all_to_all.36.got = bf16[4,112,1536]{2,1,0:T(8,128)(2,1)} all-to-all(bf16[4,112,1536]{2,1,0:T(8,128)(2,1)} %bitcast.8), channel_id=1, replica_groups=mesh['z'=16,'core'=2,'y'=8,'x'=4] {'x'}, dimensions={0} | all-to-all | bytes 2752512 | tf_op jit(solution)/shard_map/all_to_all | solution.py:227
  74.1 2.6 %shard_map.163 = bf16[128,1536]{1,0:T(8,128)(2,1)} custom-call(bf16[4,112,1536]{2,1,0:T(8,128)(2,1)} %all_to_all.36.got), custom_call_target="tpu_custom_call" | custom-call | tf_op jit(solution)/shard_map/pallas_call | solution.py:42
  76.7 21.1 %all_to_all.37.got = bf16[8,16,1536]{2,1,0:T(8,128)(2,1)} all-to-all(bf16[8,16,1536]{2,1,0:T(8,128)(2,1)} %bitcast.10), channel_id=1, replica_groups=mesh['z'=16,'core'=2,'y'=8,'x'=4] {'y'}, dimensions={0} | all-to-all | bytes 786432 | tf_op jit(solution)/shard_map/all_to_all | solution.py:227
  97.8 2.0 %shard_map.164 = bf16[8,16,1536]{2,1,0:T(8,128)(2,1)} custom-call(bf16[8,16,1536]{2,1,0:T(8,128)(2,1)} %all_to_all.37.got, bf16[32,16,256]{2,1,0:T(8,128)(2,1)} %all_to_all.35.recv), custom_call_target="tpu_custom_call" | custom-call | tf_op jit(solution)/shard_map/pallas_call | solution.py:42
  99.8 15.9 %all_to_all.38 = bf16[8,16,1536]{2,1,0:T(8,128)(2,1)S(1)} all-to-all(bf16[8,16,1536]{2,1,0:T(8,128)(2,1)} %shard_map.164), channel_id=1, replica_groups=mesh['z'=16,'core'=2,'y'=8,'x'=4] {'y'}, dimensions={0} | all-to-all | bytes 786432 | tf_op jit(solution)/shard_map/all_to_all | solution.py:227
  115.6 0.1 broadcast_in_dim.8
  115.8 20.7 %all_to_all.39 = bf16[4,128,1536]{2,1,0:T(8,128)(2,1)} all-to-all(bf16[4,128,1536]{2,1,0:T(8,128)(2,1)S(1)} %broadcast_in_dim.8), channel_id=1, replica_groups=mesh['z'=16,'core'=2,'y'=8,'x'=4] {'x'}, dimensions={0} | all-to-all | bytes 3145728 | tf_op jit(solution)/shard_map/all_to_all | solution.py:227
  136.5 3.6 %shard_map.165 = (f32[128,128]{1,0:T(8,128)}, bf16[2,16,64,128]{3,2,1,0:T(8,128)(2,1)}) custom-call(bf16[512,1536]{1,0:T(8,128)(2,1)} %bitcast.6, bf16[128,128]{1,0:T(8,128)(2,1)} %tok.5, bf16[128,128]{1,0:T(8,128)(2,1)} %cot.5, bf16[2,128,512]{2,1,0:T(8,128)(2,1)} %wg.3, bf16[2,128,512]{2,1,0:T(8,128)(2,1)} %wu.3, bf16[128,512]{1,0:T(8,128)(2,1)} %sg.3, ...), custom_call_target="tpu_custom_call" | custom-call | tf_op jit(solution)/shard_map/pallas_call | solution.py:42
  140.0 6.1 %all_to_all.40.got = bf16[2,16,64,128]{3,2,1,0:T(8,128)(2,1)} all-to-all(bf16[2,16,64,128]{3,2,1,0:T(8,128)(2,1)} %get-tuple-element.21), channel_id=1, replica_groups=mesh['z'=16,'core'=2,'y'=8,'x'=4] {'core'}, dimensions={0} | all-to-all | bytes 1048576 | tf_op jit(solution)/shard_map/all_to_all | solution.py:227
  146.1 1.8 shard_map.166
  147.9 6.0 %all-to-all-start.6 = ((bf16[16,80,128]{2,1,0:T(8,128)(2,1)}), bf16[16,80,128]{2,1,0:T(8,128)(2,1)S(1)}, u32[]{:S(2)}, u32[]{:S(2)}) async-start(bf16[16,80,128]{2,1,0:T(8,128)(2,1)} %shard_map.166), calls=%async_computation.6 | async-start | bytes 655360 | tf_op jit(solution)/shard_map/all_to_all | solution.py:227
  154.0 2.9 %shard_map.168 = (f32[2,128,512]{2,1,0:T(8,128)}, f32[2,128,512]{2,1,0:T(8,128)}, f32[2,512,128]{2,1,0:T(8,128)}) custom-call(bf16[512,1536]{1,0:T(8,128)(2,1)} %bitcast.7, bf16[32,16,256]{2,1,0:T(8,128)(2,1)} %all_to_all.35.recv), custom_call_target="tpu_custom_call" | custom-call | tf_op jit(solution)/shard_map/pallas_call | solution.py:42
  156.9 18.5 %all-to-all-done.6.got = bf16[16,80,128]{2,1,0:T(8,128)(2,1)S(1)} async-done(((bf16[16,80,128]{2,1,0:T(8,128)(2,1)}), bf16[16,80,128]{2,1,0:T(8,128)(2,1)S(1)}, u32[]{:S(2)}, u32[]{:S(2)}) %all-to-all-start.6) | async-done | bytes 327712 | tf_op jit(solution)/shard_map/all_to_all | solution.py:227
  175.3 0.0 copy-start
  175.3 0.7 copy-done
  176.1 2.1 %shard_map.167 = (bf16[128,128]{1,0:T(8,128)(2,1)}, f32[128,2]{1,0:T(8,128)}, f32[128,16]{1,0:T(8,128)}, f32[128,16]{1,0:T(8,128)}, f32[16,128]{1,0:T(8,128)}) custom-call(bf16[16,80,128]{2,1,0:T(8,128)(2,1)} %copy-done, s32[128,2]{1,0:T(8,128)} %get-tuple-element.22.ids, f32[128,128]{1,0:T(8,128)} %get-tuple-element.23.shared_grad), custom_call_target="tpu_custom_call" | custom-call | tf_op jit(solution)/shard_map/pallas_call | solution.py:42
  178.2 1.5 copy.21
  179.7 1.5 copy.22
  181.2 1.5 copy.20
Async XLA Ops:
  147.9 27.4 %all-to-all-start.6 = ((bf16[16,80,128]{2,1,0:T(8,128)(2,1)}), bf16[16,80,128]{2,1,0:T(8,128)(2,1)S(1)}, u32[]{:S(2)}, u32[]{:S(2)}) async-start(bf16[16,80,128]{2,1,0:T(8,128)(2,1)} %shard_map.166), calls=%async_computation.6 | async-start | bytes 655360 | tf_op jit(solution)/shard_map/all_to_all | solution.py:227
  175.3 0.7 copy-start

commit v2 on v1

--- a/solution.py
+++ b/solution.py
@@ -13,8 +13,8 @@
 SLOTS = 2 * CAP
 SHR = 4
 USED = SLOTS + SHR
-XROWS = NY * USED
 HID = 512
+SCALE_X, SCALE_Y = 256.0, 64.0
 
 
 def iota(shape, dim):
@@ -38,13 +38,19 @@
 
 
 def call(kernel, outs):
+    def place(o):
+        return o if isinstance(o, jax.ShapeDtypeStruct) else pltpu.VMEM(*o)
+
+    outs = [place(o) for o in outs]
+
     def run(*args):
         return pl.pallas_call(
             kernel,
             out_shape=outs,
             in_specs=[pl.BlockSpec(memory_space=pltpu.VMEM)] * len(args),
-            out_specs=jax.tree.map(lambda _: pl.BlockSpec(memory_space=pltpu.VMEM), outs),
-        )(*args)
+            out_specs=[pl.BlockSpec(memory_space=pltpu.VMEM)] * len(outs),
+            compiler_params=pltpu.CompilerParams(vmem_limit_bytes=16 << 20),
+        )(*[pltpu.with_memory_space_constraint(a, pltpu.VMEM) for a in args])
 
     return run
 
@@ -55,42 +61,37 @@
 
 def route_kernel(routes, weights, tok, cot, send, ids):
     n = tok.shape[0]
-    r0, r1 = routes[:, 0:1], routes[:, 1:2]
-    lane = iota((n, 128), 1)
-    oh0, oh1 = r0 == lane, r1 == lane
-    earlier = onehot(iota((n, n), 0) > iota((n, n), 1))
-    f0, f1 = jnp.where(oh0, 1.0, 0.0), jnp.where(oh1, 1.0, 0.0)
-    c0 = nn(earlier, f0.astype(BF))
-    c1 = nn(earlier, f1.astype(BF)) + jnp.sum(f0, axis=0, keepdims=True)
-    rank0 = jnp.sum(c0 * f0, axis=1, keepdims=True).astype(I32)
-    rank1 = jnp.sum(c1 * f1, axis=1, keepdims=True).astype(I32)
+    r0, r1 = routes[0:1, :], routes[1:2, :]
+    names = iota((NEP * 2, n), 0)
+    f0, f1 = jnp.where(r0 == names, 1.0, 0.0), jnp.where(r1 == names, 1.0, 0.0)
+    earlier = onehot(iota((n, n), 0) < iota((n, n), 1))
+    c0 = nn(f0.astype(BF), earlier)
+    c1 = nn(f1.astype(BF), earlier) + jnp.sum(f0, axis=1, keepdims=True)
+    rank0 = jnp.sum(c0 * f0, axis=0, keepdims=True).astype(I32)
+    rank1 = jnp.sum(c1 * f1, axis=0, keepdims=True).astype(I32)
     row0 = (r0 >> 1) * BLK + (r0 & 1) * CAP + rank0
     row1 = (r1 >> 1) * BLK + (r1 & 1) * CAP + rank1
-    ids[...] = jnp.where(iota((n, 2), 1) == 0, row0, row1)
-    wide = iota((n, NEP * BLK), 1)
-    places = onehot((row0 == wide) | (row1 == wide))
-    at0 = onehot((row0 >> 4) * BLK + SLOTS == wide)
-    at1 = onehot((row1 >> 4) * BLK + SLOTS == wide)
+    ids[0:1, :] = row0
+    ids[1:2, :] = row1
+    tall = iota((NEP * BLK, n), 0)
+    places = onehot((row0 == tall) | (row1 == tall))
+    send[:, 128:] = nn(places, cot[...]).astype(BF)
     gates = weights[...].astype(BF).astype(F32)
-    lane2 = iota((n, 256), 1)
-    g0 = jnp.where(lane2 == (row0 & 15), gates[:, 0:1], 0.0).astype(BF)
-    g1 = jnp.where(lane2 == (row1 & 15), gates[:, 1:2], 0.0).astype(BF)
-    feats = jnp.concatenate([tok[...], cot[...]], axis=1)
-    left = jnp.concatenate([places, at0, at1], axis=0)
-    right = jnp.concatenate([feats, g0, g1], axis=0)
-    send[...] = tn(left, right).astype(BF)
+    data = nn(places, tok[...])
+    lane = iota((n, n), 0)
+    for row, k in ((row0, 0), (row1, 1)):
+        at = jnp.where((row >> 4) * BLK + SLOTS == tall, gates[k : k + 1, :], 0.0).astype(BF)
+        data = data + nt(at, onehot(lane == (row & 15)))
+    send[:, :128] = data.astype(BF)
 
 
 def partial_kernel(recv, tok, cot, wg, wu, wd, sg, su, sd, out):
-    rows = NX * XROWS
-    r = iota((rows, 1), 0)
-    x = (r * 293) >> 15
-    rest = r - x * XROWS
-    y = (rest * 293) >> 12
-    q = rest - y * USED
-    s = y * NX + x
+    r = iota((NTP * BLK, 1), 0)
+    q = r & 15
+    s = ((r >> 4) & (NY - 1)) * NX + (r >> 7)
     src = jnp.where(q < SLOTS, s * BLK + q, NEP * BLK + s * SHR + q - SLOTS)
-    pick = onehot(src == iota((rows, NEP * BLK + 128), 1))
+    src = jnp.where(q < USED, src, -1)
+    pick = onehot(src == iota((NTP * BLK, NEP * BLK + 128), 1))
     feats = jnp.concatenate([tok[...], cot[...]], axis=1)
     data = nn(pick, jnp.concatenate([recv[...], feats], axis=0))
     kinds = (q < CAP, (q >= CAP) & (q < SLOTS), q >= SLOTS)
@@ -98,30 +99,16 @@
     tcat = jnp.concatenate([jnp.where(k, t, 0.0).astype(BF) for k in kinds], axis=1)
     ccat = jnp.concatenate([jnp.where(k, c, 0.0).astype(BF) for k in kinds], axis=1)
     wgc = jnp.concatenate([wg[0], wg[1], sg[...]], axis=0)
-    out[:, :HID] = nn(tcat, wgc).astype(BF)
+    out[:, :HID] = nn(tcat, wgc) * SCALE_X
     wuc = jnp.concatenate([wu[0], wu[1], su[...]], axis=0)
-    out[:, HID : 2 * HID] = nn(tcat, wuc).astype(BF)
+    out[:, HID : 2 * HID] = nn(tcat, wuc) * SCALE_X
     wdc = jnp.concatenate([wd[0], wd[1], sd[...]], axis=1)
-    out[:, 2 * HID :] = nt(ccat, wdc).astype(BF)
-
-
-def middle_kernel(got, out):
-    o = iota((NY * BLK, 1), 0)
-    q = o & 15
-    want = jnp.where(q < USED, (o >> 4) * USED + q, -1)
-    r = iota((NY * BLK, XROWS), 1)
-    pick = onehot(want == r)
-    total = nn(pick, got[0])
-    for k in range(1, NX):
-        total = total + nn(pick, got[k])
-    out[...] = total.astype(BF)
+    out[:, 2 * HID :] = nt(ccat, wdc) * SCALE_X
 
 
 def hidden_kernel(got, recv, out):
     t = lax.axis_index("y") * NX + lax.axis_index("x")
-    pre = got[0].astype(F32)
-    for k in range(1, NY):
-        pre = pre + got[k].astype(F32)
+    pre = got[...] * (1.0 / SCALE_Y)
     gate, up, back = pre[:, :HID], pre[:, HID : 2 * HID], pre[:, 2 * HID :]
     q = iota((BLK, 1), 0)
     lane = iota((BLK, 128), 1)
@@ -200,27 +187,25 @@
 
 
 def final_kernel(got, ids, shared_grad, grad_tokens, grad_weights, og, ou, od):
-    n = ids.shape[0]
-    row0, row1 = ids[:, 0:1], ids[:, 1:2]
+    n = ids.shape[1]
+    row0, row1 = ids[0:1, :], ids[1:2, :]
     back = jnp.concatenate([got[z, : 2 * BLK] for z in range(NZ)], axis=0)
-    wide = iota((n, NEP * BLK), 1)
-    places = onehot((row0 == wide) | (row1 == wide))
-    grad_tokens[...] = (nn(places, back) + shared_grad[...]).astype(BF)
-    lane = iota((n, 128), 1)
-    sums = []
-    for row in (row0, row1):
+    tall = iota((NEP * BLK, n), 0)
+    places = onehot((row0 == tall) | (row1 == tall))
+    grad_tokens[...] = (tn(places, back) + shared_grad[...]).astype(BF)
+    lane = iota((n, n), 0)
+    for row, k in ((row0, 0), (row1, 1)):
         base = (row >> 4) * BLK + USED
-        line = nn(onehot((wide == base) | (wide == base + 1)), back)
-        sums.append(jnp.sum(jnp.where(lane == (row & 15), line, 0.0), axis=1, keepdims=True))
-    grad_weights[...] = jnp.where(iota((n, 2), 1) == 0, sums[0], sums[1])
+        line = tn(back, onehot((tall == base) | (tall == base + 1)))
+        grad_weights[k : k + 1, :] = jnp.sum(
+            jnp.where(lane == (row & 15), line, 0.0), axis=0, keepdims=True
+        )
     total = got[0, 2 * BLK :].astype(F32)
     for z in range(1, NZ):
         total = total + got[z, 2 * BLK :].astype(F32)
+    og[...] = total[:BLK]
+    ou[...] = total[BLK : 2 * BLK]
     od[...] = total[2 * BLK :]
-    pad = jnp.zeros((128 - 2 * BLK, 128), F32)
-    turned = jnp.concatenate([total[: 2 * BLK], pad], axis=0).T
-    og[...] = turned[:, :BLK]
-    ou[...] = turned[:, BLK : 2 * BLK]
 
 
 def swap(array, axis):
@@ -229,41 +214,43 @@
 
 def body(tok, routes, weights, cot, wg, wu, wd, sg, su, sd):
     n, feats = tok.shape
-    send, ids = call(
-        route_kernel, (struct((NEP * BLK, 2 * feats), BF), struct((n, 2), I32))
-    )(routes, weights, tok, cot)
+    wide = 3 * HID
+    send, ids = call(route_kernel, [((NEP * BLK, 2 * feats), BF), ((2, n), I32)])(
+        routes.T, weights.T, tok, cot
+    )
     recv = swap(send.reshape(NEP, BLK, 2 * feats), ("z", "core"))
-    part = call(partial_kernel, struct((NX * XROWS, 3 * HID), BF))(
+    (part,) = call(partial_kernel, [((NTP * BLK, wide), F32)])(
         recv.reshape(NEP * BLK, 2 * feats), tok, cot, wg, wu, wd, sg, su, sd
     )
-    got = swap(part.reshape(NX, XROWS, 3 * HID), "x")
-    mid = call(middle_kernel, struct((NY * BLK, 3 * HID), BF))(got)
-    got = swap(mid.reshape(NY, BLK, 3 * HID), "y")
-    grads = call(hidden_kernel, struct((NY, BLK, 3 * HID), BF))(got, recv)
-    grads = swap(grads, "y").reshape(1, NY * BLK, 3 * HID)
-    grads = swap(jnp.broadcast_to(grads, (NX, NY * BLK, 3 * HID)), "x")
-    grads = grads.reshape(NTP * BLK, 3 * HID)
+    got = swap(part.astype(jnp.float16).reshape(NX, NY * BLK, wide), "x")
+    mid = jnp.sum(got.astype(F32), axis=0) * (SCALE_Y / SCALE_X)
+    got = swap(mid.astype(jnp.float16).reshape(NY, BLK, wide), "y")
+    pre = jnp.sum(got.astype(F32), axis=0)
+    (grads,) = call(hidden_kernel, [((NY, BLK, wide), BF)])(pre, recv)
+    grads = swap(grads, "y").reshape(1, NY * BLK, wide)
+    grads = swap(jnp.broadcast_to(grads, (NX, NY * BLK, wide)), "x")
+    grads = grads.reshape(NTP * BLK, wide)
     shared_grad, back = call(
-        back_kernel, (struct((n, feats), F32), struct((NC, NZ, 4 * BLK, feats), BF))
+        back_kernel, [((n, feats), F32), ((NC, NZ, 4 * BLK, feats), BF)]
     )(grads, tok, cot, wg, wu, sg, su)
     back = swap(back, "core")
-    back = call(core_kernel, struct((NZ, 5 * BLK, feats), BF))(back)
+    (back,) = call(core_kernel, [((NZ, 5 * BLK, feats), BF)])(back)
     back = swap(back, "z")
     grad_g, grad_u, grad_d = call(
         weights_kernel,
-        (struct((2, feats, HID), F32), struct((2, feats, HID), F32), struct((2, HID, feats), F32)),
+        [struct((2, feats, HID), F32), struct((2, feats, HID), F32), struct((2, HID, feats), F32)],
     )(grads, recv)
     grad_tokens, grad_weights, shared_g, shared_u, shared_d = call(
         final_kernel,
-        (
+        [
             struct((n, feats), BF),
-            struct((n, 2), F32),
-            struct((feats, BLK), F32),
-            struct((feats, BLK), F32),
+            struct((2, n), F32),
             struct((BLK, feats), F32),
-        ),
+            struct((BLK, feats), F32),
+            struct((BLK, feats), F32),
+        ],
     )(back, ids, shared_grad)
-    return grad_tokens, grad_weights, grad_g, grad_u, grad_d, shared_g, shared_u, shared_d
+    return grad_tokens, grad_weights.T, grad_g, grad_u, grad_d, shared_g.T, shared_u.T, shared_d
 
 
 def solution(mesh):

time: 184 us -> 170 us (0.924)
  Pallas kernels: 21.4 us -> 6.58 us
  blocking collectives: 128 us -> 126 us
  local copies, waits for them, and re-layouts: 8.17 us -> 10.1 us
    pallas_call x8 -> x7, Pallas kernels: 21.4 us -> 6.58 us  [run(): pl.pallas_call(kernel, out_shape=outs, in_specs=[pl.BlockSpec(memory_spac...]
    all_to_all x6, blocking collectives: 128 us -> 126 us  [swap(): return lax.all_to_all(array, axis, 0, 0, tiled=True)]
    unnamed x7 -> x36, local copies, waits for them, and re-layouts: 8.05 us -> 9.98 us
  transfers between devices with their start and end apart: 1 -> 1, of which waited for: 1 -> 1; matrix products, arithmetic and copies ran while one was open for 0% -> 0% of each run, Pallas kernels for 2% -> 1%
where the time goes in v2:
time: 170 us; the launch traced here: 169 us
  blocking collectives  126 us (74%)
  waiting for transfers between devices  19.9 us (12%)
  local copies, waits for them, and re-layouts  10.1 us (6%)
  Pallas kernels  6.58 us (4%)
  starting transfers between devices  4.94 us (3%)
    all_to_all x6, blocking collectives, swap(): return lax.all_to_all(array, axis, 0, 0, tiled=True)  126 us
    all_to_all x1, waiting for transfers between devices, swap(): return lax.all_to_all(array, axis, 0, 0, tiled=True)  19.9 us
    unnamed x36, local copies, waits for them, and re-layouts  9.98 us
    pallas_call x7, Pallas kernels, run(): pl.pallas_call(kernel, out_shape=outs, in_specs=[pl.BlockSpec(memory_spac...  6.58 us
    all_to_all x1, starting transfers between devices, swap(): return lax.all_to_all(array, axis, 0, 0, tiled=True)  4.94 us
  transfers between devices with their start and end apart: 1, of which 1 were waited for; matrix products, arithmetic and copies ran while one was open for 0% of the time, Pallas kernels for 1%

profile of v2, /device:TPU:2, one launch (start us, length us, event | category | flops | bytes accessed | tf_op | source)
XLA Modules:
  0.0 168.7 jit_solution(14798548631858485556)
XLA Ops:
  0.6 0.7 copy-done.8
  1.4 0.8 copy-done.11
  2.2 0.7 copy-done.16
  4.0 41.6 %all_to_all.35.recv = bf16[32,16,256]{2,1,0:T(8,128)(2,1)S(1)} all-to-all(bf16[32,16,256]{2,1,0:T(8,128)(2,1)S(1)} %bitcast.14), channel_id=1, replica_groups=mesh['z'=16,'core'=2,'y'=8,'x'=4] {'z','core'}, dimensions={0} | all-to-all | bytes 524288 | tf_op jit(solution)/shard_map/all_to_all | solution.py:212
  45.6 0.9 copy-done
  46.6 0.9 copy-done.2
  47.5 0.9 copy-done.4
  48.4 0.9 copy-done.6
  49.4 0.8 copy-done.9
  50.1 0.8 copy-done.12
  50.9 0.9 copy-done.14
  51.8 0.9 copy-done.15
  52.7 1.6 shard_map.162
  54.6 23.9 %all_to_all.36 = f16[4,128,1536]{2,1,0:T(8,128)(2,1)S(1)} all-to-all(f16[4,128,1536]{2,1,0:T(8,128)(2,1)S(1)} %bitcast.17), channel_id=1, replica_groups=mesh['z'=16,'core'=2,'y'=8,'x'=4] {'x'}, dimensions={0} | all-to-all | bytes 3145728 | tf_op jit(solution)/shard_map/all_to_all | solution.py:212
  78.8 20.5 %all_to_all.37 = f16[8,16,1536]{2,1,0:T(8,128)(2,1)S(1)} all-to-all(f16[8,16,1536]{2,1,0:T(8,128)(2,1)S(1)} %bitcast.18), channel_id=1, replica_groups=mesh['z'=16,'core'=2,'y'=8,'x'=4] {'y'}, dimensions={0} | all-to-all | bytes 786432 | tf_op jit(solution)/shard_map/all_to_all | solution.py:212
  99.5 15.5 %all_to_all.38 = bf16[8,16,1536]{2,1,0:T(8,128)(2,1)S(1)} all-to-all(bf16[8,16,1536]{2,1,0:T(8,128)(2,1)S(1)} %shard_map.163), channel_id=1, replica_groups=mesh['z'=16,'core'=2,'y'=8,'x'=4] {'y'}, dimensions={0} | all-to-all | bytes 786432 | tf_op jit(solution)/shard_map/all_to_all | solution.py:212
  115.2 20.2 %all_to_all.39 = bf16[4,128,1536]{2,1,0:T(8,128)(2,1)S(1)} all-to-all(bf16[4,128,1536]{2,1,0:T(8,128)(2,1)S(1)} %broadcast_in_dim.8), channel_id=1, replica_groups=mesh['z'=16,'core'=2,'y'=8,'x'=4] {'x'}, dimensions={0} | all-to-all | bytes 3145728 | tf_op jit(solution)/shard_map/all_to_all | solution.py:212
  135.4 1.1 shard_map.164
  136.6 4.2 %all_to_all.40.got = bf16[2,16,64,128]{3,2,1,0:T(8,128)(2,1)S(1)} all-to-all(bf16[2,16,64,128]{3,2,1,0:T(8,128)(2,1)S(1)} %get-tuple-element.21), channel_id=1, replica_groups=mesh['z'=16,'core'=2,'y'=8,'x'=4] {'core'}, dimensions={0} | all-to-all | bytes 1048576 | tf_op jit(solution)/shard_map/all_to_all | solution.py:212
  140.7 0.8 shard_map.165
  141.5 4.9 %all-to-all-start.6 = ((bf16[16,80,128]{2,1,0:T(8,128)(2,1)}), bf16[16,80,128]{2,1,0:T(8,128)(2,1)S(1)}, u32[]{:S(2)}, u32[]{:S(2)}) async-start(bf16[16,80,128]{2,1,0:T(8,128)(2,1)} %shard_map.165), calls=%async_computation.6 | async-start | bytes 655360 | tf_op jit(solution)/shard_map/all_to_all | solution.py:212
  146.4 1.5 shard_map.167
  147.9 19.9 %all-to-all-done.6.got = bf16[16,80,128]{2,1,0:T(8,128)(2,1)S(1)} async-done(((bf16[16,80,128]{2,1,0:T(8,128)(2,1)}), bf16[16,80,128]{2,1,0:T(8,128)(2,1)S(1)}, u32[]{:S(2)}, u32[]{:S(2)}) %all-to-all-start.6) | async-done | bytes 327712 | tf_op jit(solution)/shard_map/all_to_all | solution.py:212
  167.8 0.9 shard_map.166
  (32 shorter events, 2.1 us)
Async XLA Ops:
  0.6 0.8 copy-start.8
  1.4 0.8 copy-start.11
  2.2 0.7 copy-start.16
  2.8 0.7 copy-start.17
  45.6 1.0 copy-start
  46.6 0.9 copy-start.2
  47.5 0.9 copy-start.4
  48.4 0.9 copy-start.6
  49.3 0.8 copy-start.9
  50.1 0.8 copy-start.12
  50.9 0.9 copy-start.14
  51.8 0.9 copy-start.15
  115.1 20.3 %copy-start.1 = (bf16[2,128,512]{2,1,0:T(8,128)(2,1)S(1)}, bf16[2,128,512]{2,1,0:T(8,128)(2,1)}, u32[]{:S(2)}) copy-start(bf16[2,128,512]{2,1,0:T(8,128)(2,1)} %wg.3) | copy-start | bytes 786436
  115.1 20.2 %copy-start.3 = (bf16[2,128,512]{2,1,0:T(8,128)(2,1)S(1)}, bf16[2,128,512]{2,1,0:T(8,128)(2,1)}, u32[]{:S(2)}) copy-start(bf16[2,128,512]{2,1,0:T(8,128)(2,1)} %wu.3) | copy-start | bytes 786436
  115.1 20.2 %copy-start.5 = (bf16[128,512]{1,0:T(8,128)(2,1)S(1)}, bf16[128,512]{1,0:T(8,128)(2,1)}, u32[]{:S(2)}) copy-start(bf16[128,512]{1,0:T(8,128)(2,1)} %sg.3) | copy-start | bytes 393220
  115.1 20.2 %copy-start.7 = (bf16[128,512]{1,0:T(8,128)(2,1)S(1)}, bf16[128,512]{1,0:T(8,128)(2,1)}, u32[]{:S(2)}) copy-start(bf16[128,512]{1,0:T(8,128)(2,1)} %su.3) | copy-start | bytes 393220
  115.2 20.2 %copy-start.10 = (bf16[128,128]{1,0:T(8,128)(2,1)S(1)}, bf16[128,128]{1,0:T(8,128)(2,1)}, u32[]{:S(2)}) copy-start(bf16[128,128]{1,0:T(8,128)(2,1)} %tok.5) | copy-start | bytes 98308
  115.2 20.2 %copy-start.13 = (bf16[128,128]{1,0:T(8,128)(2,1)S(1)}, bf16[128,128]{1,0:T(8,128)(2,1)}, u32[]{:S(2)}) copy-start(bf16[128,128]{1,0:T(8,128)(2,1)} %cot.5) | copy-start | bytes 98308
  141.5 26.3 %all-to-all-start.6 = ((bf16[16,80,128]{2,1,0:T(8,128)(2,1)}), bf16[16,80,128]{2,1,0:T(8,128)(2,1)S(1)}, u32[]{:S(2)}, u32[]{:S(2)}) async-start(bf16[16,80,128]{2,1,0:T(8,128)(2,1)} %shard_map.165), calls=%async_computation.6 | async-start | bytes 655360 | tf_op jit(solution)/shard_map/all_to_all | solution.py:212
